TPU v7x, 512 devices: a 4x2x32 block of a 4x8x32 slice. The times are simulated.
512 devices in a mesh: grp: 2 (over y), sp: 64 (over z, core), tp: 4 (over x).
Axes of the slice: x: 4, y: 2, z: 32, core: 2. Of those that a mesh axis runs over, the one named last changes fastest.
The devices are a block of a 4x8x32 slice.
Arguments:
- tokens: bfloat16 [49152, 2048], P(('grp', 'sp')), parts along dimension 0, may hold values from -6 to 6
- norm_gain: float32 [2, 2048], replicated, may hold values from 0.1 to 1.9
- entry_weight: bfloat16 [2, 2048, 2048], P(None, 'sp', 'tp'), may hold values from -0.125 to 0.125
- mix_weight: bfloat16 [2, 4, 512, 512], P(None, 'tp'), may hold values from -0.25 to 0.25
- pool_gain: float32 [2, 2048], P(None, 'tp'), may hold values from 0.1 to 1.9
- back_weight: bfloat16 [2, 2048, 2048], P(None, 'tp', 'sp'), may hold values from -0.25 to 0.25
Outputs:
- result_tokens: bfloat16 [49152, 2048], P(('grp', 'sp')), parts along dimension 0
There are 2 independent parts, one for each index of `grp`. A program takes and returns all parts, laid end to end along the dimension named above; an argument that names none is the same for every part. Nothing has to cross between parts.
All inputs are finite; a program needn't handle non-finite values.
Results may differ from a plain program's by a relative error of at most 0.018.
Values may be sent and summed in bfloat16 or wider, within the bound.
A program may use at most 64 MiB of HBM per device.

v0:
```python
import jax
import jax.numpy as jnp
from jax import lax
from jax.sharding import PartitionSpec as P

GROUPS = 4
LAYERS = 2
EPSILON = 1e-05


def extended_2(value, sides, width):
    for axis, dim in sides:
        size, length = (lax.axis_size(axis), value.shape[dim])
        up = [(i, (i + 1) % size) for i in range(size - 1)]
        down = [(j, i) for i, j in up]
        last = lax.slice_in_dim(value, length - width, length, axis=dim)
        first = lax.slice_in_dim(value, 0, width, axis=dim)
        before = lax.ppermute(last, axis, up)
        after = lax.ppermute(first, axis, down)
        value = jnp.concatenate([before, value, after], axis=dim)
    return value


def gather_turned(arrays, axis, dims):
    turned = [jnp.moveaxis(a, dim, 0) for a, dim in zip(arrays, dims)]
    both = jnp.concatenate([t.reshape(len(t), -1) for t in turned], axis=1)
    out, at, done = (lax.all_gather(both, axis, axis=0, tiled=True), 0, [])
    for t, dim in zip(turned, dims):
        section = out[:, at : at + t[0].size].reshape(-1, *t.shape[1:])
        done.append(jnp.moveaxis(section, 0, dim))
        at += t[0].size
    return tuple(done)


def from_everyone(value, axis):
    length = lax.axis_size(axis)
    return lax.all_to_all(
        jnp.broadcast_to(value[None], (length, *value.shape)), axis, 0, 0, tiled=True
    )


def over_copies(value, axis):
    everything = from_everyone(value, axis)
    return jnp.sum(everything.astype(jnp.float32), axis=0)


def window_mean(padded, positions, halves, total_length, reach):
    row_count = positions.shape[0]
    summed = jnp.zeros((row_count,) + padded.shape[1:], jnp.float32)
    for offset in range(-reach, reach):
        inside = ((offset >= -halves) & (offset < halves)).astype(jnp.float32)
        summed = (
            summed + padded[reach + offset : reach + offset + row_count] * inside[None, :, None]
        )
    lower = jnp.maximum(positions[:, None] - halves[None, :], 0)
    upper = jnp.minimum(positions[:, None] + halves[None, :], total_length)
    counted = (upper - lower).astype(jnp.float32)
    return summed / counted[:, :, None]


def normalize(state, gain):
    values = state.astype(jnp.float32)
    scaled = values * lax.rsqrt(jnp.mean(values * values, axis=-1, keepdims=True) + EPSILON)
    return (scaled * gain).astype(jnp.bfloat16)


def pool_groups(pooled_in, mix_layer, gain_layer, reach):
    row_count = pooled_in.shape[0]
    group_here = mix_layer.shape[0]
    width = mix_layer.shape[1]
    extended = extended_2(pooled_in, (("sp", 0),), reach)
    first_group = lax.axis_index("tp") * group_here
    halves = jnp.left_shift(jnp.int32(1), first_group + jnp.arange(group_here, dtype=jnp.int32))
    positions = lax.axis_index("sp") * row_count + jnp.arange(row_count, dtype=jnp.int32)
    total_length = lax.axis_size("sp") * row_count
    padded = extended.reshape(row_count + 2 * reach, group_here, width).astype(jnp.float32)
    means = window_mean(padded, positions, halves, total_length, reach)
    differ = (means - padded[reach : reach + row_count]).astype(jnp.bfloat16)
    mixed = jnp.einsum("tgc,gcd->tgd", differ, mix_layer, preferred_element_type=jnp.float32)
    return (mixed.reshape(row_count, group_here * width) * gain_layer).astype(jnp.bfloat16)


def per_device(tokens, norm_gain, entry_weight, mix_weight, pool_gain, back_weight):
    reach = 2 ** (GROUPS - 1)
    state = tokens
    entry_all, back_all = gather_turned((entry_weight, back_weight), "sp", (1, 2))
    for layer in range(LAYERS):
        normed = normalize(state, norm_gain[layer])
        pooled_in = jnp.dot(normed, entry_all[layer], preferred_element_type=jnp.float32).astype(
            jnp.bfloat16
        )
        back_local = back_all[layer]
        mixed = pool_groups(pooled_in, mix_weight[layer], pool_gain[layer], reach)
        update = jnp.dot(mixed, back_local, preferred_element_type=jnp.float32)
        summed = over_copies(update.astype(jnp.bfloat16), "tp").astype(jnp.float32)
        state = (state.astype(jnp.float32) + summed).astype(jnp.bfloat16)
    return state


def solution(mesh):
    return jax.shard_map(
        per_device,
        mesh=mesh,
        in_specs=(
            P(("grp", "sp"), None),
            P(),
            P(None, "sp", "tp"),
            P(None, "tp", None, None),
            P(None, "tp"),
            P(None, "tp", "sp"),
        ),
        out_specs=P(("grp", "sp"), None),
        check_vma=False,
    )
```

profile of v0, /device:TPU:33, one launch (start us, length us, event | category | flops | bytes accessed | tf_op | source)
XLA Modules:
  0.0 392.6 jit_solution(11383457933430418808)
XLA Ops:
  6.5 0.0 all-gather.2.cloned.1.call-start
  6.6 0.8 copy.17
  7.4 0.8 copy.18
  8.2 0.7 pad_maximum_fusion
  8.9 0.1 all-gather.2.cloned.1.call-update
  9.0 1.8 fusion
  10.8 0.8 fusion.87
  11.6 0.8 fusion.86
  12.4 164.7 %all-gather.2.cloned.1.call-done = bf16[2048,2048]{1,0:T(8,128)(2,1)} async-done(((bf16[32,2048]{1,0:T(8,128)(2,1)}), bf16[2048,2048]{1,0:T(8,128)(2,1)}) %all-gather.2.cloned.1.call-update) | async-done | bytes 8388624 | tf_op jit(solution)/shard_map/all_gather | solution.py:27
  177.1 5.2 %fusion.83 = (bf16[2048,1024]{1,0:T(8,128)(2,1)S(1)}, bf16[2048,1024]{1,0:T(8,128)(2,1)}) fusion(bf16[2048,2048]{1,0:T(8,128)(2,1)} %all-gather.2.cloned.1.call-done), kind=kLoop, calls=%fused_computation.119 | loop fusion | bytes 16777216 | tf_op jit(solution)/shard_map/slice | solution.py:29
  182.3 0.0 copy-start
  182.3 0.3 copy.20
  182.6 0.0 copy-start.1
  182.6 1.3 copy-done
  184.0 1.0 fusion.20
  185.0 0.0 copy-done.1
  185.0 2.0 collective-permute-start
  187.0 2.4 collective-permute-start.1
  189.5 6.6 %copy.15 = bf16[2048,1024]{0,1:T(8,128)(2,1)} copy(bf16[2048,1024]{1,0:T(8,128)(2,1)} %get-tuple-element.8) | data formatting | bytes 8388608 | tf_op jit(solution)/shard_map/reshape | solution.py:29
  196.1 0.0 collective-permute-done
  196.1 0.0 collective-permute-done.1
  196.1 1.0 maximum_convert_fusion
  197.1 11.0 %convolution_convert_fusion.1 = bf16[384,2048]{1,0:T(8,128)(2,1)S(1)} fusion(bf16[2,512,2048]{2,1,0:T(8,128)(2,1)} %bitcast.97, bf16[2,1,512,512]{3,2,1,0:T(8,128)(2,1)} %param.9, f32[512]{0:T(512)S(1)} %bitcast.112, f32[400,1,512]{2,0,1:T(8,128)} %maximum_convert_fusion, f32[384]{0:T(512)S(1)} %subtract_convert_fusion, f32[]{:T(128)S(6)} %mul.373, ...), kind=kOutput, calls=%fused_computation.18 | convolution fusion | flops 1014497280 | bytes 16780864 | tf_op jit(solution)/shard_map/dot_general | solution.py:94
  208.1 0.8 broadcast_in_dim.4
  208.9 75.3 %all_to_all.10 = bf16[4,384,2048]{2,1,0:T(8,128)(2,1)S(1)} all-to-all(bf16[4,384,2048]{2,1,0:T(8,128)(2,1)S(1)} %broadcast_in_dim.4), channel_id=1, replica_groups=mesh['grp'=2,'sp'=64,'tp'=4] {'tp'}, dimensions={0} | all-to-all | bytes 12582912 | tf_op jit(solution)/shard_map/all_to_all | solution.py:37
  284.2 1.3 convert_reduce_fusion.1
  285.5 0.0 copy-start.2
  285.5 0.5 fusion.4
  286.1 1.6 copy-done.2
  287.7 1.0 fusion.23
  288.7 3.5 collective-permute-start.2
  292.2 2.1 collective-permute-start.3
  294.4 0.0 collective-permute-done.2
  294.4 2.9 collective-permute-done.3
  297.2 1.0 maximum_convert_fusion.1
  298.2 11.0 %convolution_convert_fusion = bf16[384,2048]{1,0:T(8,128)(2,1)S(1)} fusion(bf16[2,512,2048]{2,1,0:T(8,128)(2,1)} %bitcast.98, bf16[2,1,512,512]{3,2,1,0:T(8,128)(2,1)} %param.9, f32[512]{0:T(512)S(1)} %bitcast.111, f32[400,1,512]{2,0,1:T(8,128)} %maximum_convert_fusion.1, f32[384]{0:T(512)S(1)} %subtract_convert_fusion, f32[]{:T(128)S(6)} %mul.373, ...), kind=kOutput, calls=%fused_computation.17 | convolution fusion | flops 1014497280 | bytes 16780864 | tf_op jit(solution)/shard_map/dot_general | solution.py:94
  309.2 0.8 broadcast_in_dim.5
  310.0 72.8 %all_to_all.11 = bf16[4,384,2048]{2,1,0:T(8,128)(2,1)S(1)} all-to-all(bf16[4,384,2048]{2,1,0:T(8,128)(2,1)S(1)} %broadcast_in_dim.5), channel_id=1, replica_groups=mesh['grp'=2,'sp'=64,'tp'=4] {'tp'}, dimensions={0} | all-to-all | bytes 12582912 | tf_op jit(solution)/shard_map/all_to_all | solution.py:37
  382.8 1.3 convert_reduce_fusion
  384.1 1.6 fusion.7
  (5 shorter events, 0.0 us)
Async XLA Ops:
  6.5 170.5 %all-gather.2.cloned.1.call-start = ((), (), s32[]{:S(2)}) async-start(), calls=%async_computation.2 | async-start | bytes 8519680 | tf_op jit(solution)/shard_map/all_gather | solution.py:27
  182.3 1.7 copy-start
  182.6 2.4 copy-start.1
  185.0 11.1 %collective-permute-start = (bf16[8,512]{1,0:T(8,128)(2,1)S(1)}, bf16[8,512]{1,0:T(8,128)(2,1)S(1)}, u32[]{:S(2)}, u32[]{:S(2)}) collective-permute-start(bf16[8,512]{1,0:T(8,128)(2,1)S(1)} %get-tuple-element.11), channel_id=1, source_target_pairs={{0,4},{4,8},{8,12},{12,16},{16,20},{20,24},{24,28},{28,32},{32,36}... | collective-permute-start | bytes 24584 | tf_op jit(solution)/shard_map/ppermute | solution.py:18
  187.0 9.1 %collective-permute-start.1 = (bf16[8,512]{1,0:T(8,128)(2,1)S(1)}, bf16[8,512]{1,0:T(8,128)(2,1)S(1)}, u32[]{:S(2)}, u32[]{:S(2)}) collective-permute-start(bf16[8,512]{1,0:T(8,128)(2,1)S(1)} %get-tuple-element.12), channel_id=1, source_target_pairs={{4,0},{8,4},{12,8},{16,12},{20,16},{24,20},{28,24},{32,28},{36,32}... | collective-permute-start | bytes 24584 | tf_op jit(solution)/shard_map/ppermute | solution.py:19
  285.5 2.2 copy-start.2
  288.7 5.6 %collective-permute-start.2 = (bf16[8,512]{1,0:T(8,128)(2,1)S(1)}, bf16[8,512]{1,0:T(8,128)(2,1)S(1)}, u32[]{:S(2)}, u32[]{:S(2)}) collective-permute-start(bf16[8,512]{1,0:T(8,128)(2,1)S(1)} %get-tuple-element.9), channel_id=1, source_target_pairs={{0,4},{4,8},{8,12},{12,16},{16,20},{20,24},{24,28},{28,32},{32,36}... | collective-permute-start | bytes 24584 | tf_op jit(solution)/shard_map/ppermute | solution.py:18
  292.2 5.0 %collective-permute-start.3 = (bf16[8,512]{1,0:T(8,128)(2,1)S(1)}, bf16[8,512]{1,0:T(8,128)(2,1)S(1)}, u32[]{:S(2)}, u32[]{:S(2)}) collective-permute-start(bf16[8,512]{1,0:T(8,128)(2,1)S(1)} %get-tuple-element.10), channel_id=1, source_target_pairs={{4,0},{8,4},{12,8},{16,12},{20,16},{24,20},{28,24},{32,28},{36,32}... | collective-permute-start | bytes 24584 | tf_op jit(solution)/shard_map/ppermute | solution.py:19
Sparse Core Ops, SparseCore 0:
  9.5 167.5 all-gather.1
where the time goes:
time: 393 us
  waiting for transfers between devices  168 us (43%)
  blocking collectives  148 us (38%)
  matrix products  24 us (6%)
  local copies, waits for them, and re-layouts  19.9 us (5%)
  between operations  13.7 us (3%)
  starting transfers between devices  9.98 us (3%)
  other arithmetic  9.18 us (2%)
    all_gather x1, waiting for transfers between devices, gather_turned(): out, at, done = (lax.all_gather(both, axis, axis=0, tiled=True), 0, [])  165 us
    all_to_all x2, blocking collectives, from_everyone(): lax.all_to_all(jnp.broadcast_to(value[None], (length, *value.shape)), axi...  148 us
    dot_general x2, matrix products, per_device(): update = jnp.dot(mixed, back_local, preferred_element_type=jnp.float32)  22 us
  transfers between devices with their start and end apart: 5, of which 2 were waited for; matrix products, arithmetic and copies ran while one was open for 3% of the time, Pallas kernels for 0%

commit v1 on v0

--- a/solution.py
+++ b/solution.py
@@ -24,7 +24,13 @@
 def gather_turned(arrays, axis, dims):
     turned = [jnp.moveaxis(a, dim, 0) for a, dim in zip(arrays, dims)]
     both = jnp.concatenate([t.reshape(len(t), -1) for t in turned], axis=1)
-    out, at, done = (lax.all_gather(both, axis, axis=0, tiled=True), 0, [])
+    out, at, done = (
+        jnp.concatenate(
+            lax.all_to_all(jnp.stack([both] * lax.axis_size(axis)), axis, 0, 0), axis=0
+        ),
+        0,
+        [],
+    )
     for t, dim in zip(turned, dims):
         section = out[:, at : at + t[0].size].reshape(-1, *t.shape[1:])
         done.append(jnp.moveaxis(section, 0, dim))

time: 393 us -> 1010 us (2.57)
  waiting for transfers between devices: 168 us -> 728 us
  starting transfers between devices: 9.98 us -> 68.9 us
  between operations: 13.7 us -> 0.32 us
    all_to_all x0 -> x1, waiting for transfers between devices: none -> 726 us  [gather_turned(): lax.all_to_all(jnp.stack([both] * lax.axis_size(axis)), axis, 0, 0)]
    all_gather x1 -> x0, waiting for transfers between devices: 165 us -> none  [gather_turned(): out, at, done = (lax.all_gather(both, axis, axis=0, tiled=True), 0, [])]
    all_to_all x0 -> x1, starting transfers between devices: none -> 47.6 us  [gather_turned(): lax.all_to_all(jnp.stack([both] * lax.axis_size(axis)), axis, 0, 0)]
  transfers between devices with their start and end apart: 5 -> 5, of which waited for: 2 -> 2; matrix products, arithmetic and copies ran while one was open for 3% -> 1% of each run, Pallas kernels for 0% -> 0%
where the time goes in v1:
time: 1010 us
  waiting for transfers between devices  728 us (72%)
  blocking collectives  149 us (15%)
  starting transfers between devices  68.9 us (7%)
  local copies, waits for them, and re-layouts  28.2 us (3%)
  matrix products  24.9 us (2%)
    all_to_all x1, waiting for transfers between devices, gather_turned(): lax.all_to_all(jnp.stack([both] * lax.axis_size(axis)), axis, 0, 0)  726 us
    all_to_all x2, blocking collectives, from_everyone(): lax.all_to_all(jnp.broadcast_to(value[None], (length, *value.shape)), axi...  149 us
    all_to_all x1, starting transfers between devices, gather_turned(): lax.all_to_all(jnp.stack([both] * lax.axis_size(axis)), axis, 0, 0)  47.6 us
    dot_general x2, matrix products, per_device(): update = jnp.dot(mixed, back_local, preferred_element_type=jnp.float32)  21.2 us
  transfers between devices with their start and end apart: 5, of which 2 were waited for; matrix products, arithmetic and copies ran while one was open for 1% of the time, Pallas kernels for 0%

profile of v1, /device:TPU:33, one launch (start us, length us, event | category | flops | bytes accessed | tf_op | source)
XLA Modules:
  0.0 1006.6 jit_solution(559730007724326502)
XLA Ops:
  0.0 0.8 copy.23
  0.8 0.8 copy.24
  1.7 4.3 stack.2
  6.0 0.0 copy-start
  6.0 0.0 copy-start.3
  6.0 0.0 copy-start.2
  6.0 47.6 %all-to-all-start = ((bf16[64,32,2048]{2,1,0:T(8,128)(2,1)}), bf16[64,32,2048]{2,1,0:T(8,128)(2,1)}, u32[]{:S(2)}, u32[]{:S(2)}) async-start(bf16[64,32,2048]{2,1,0:T(8,128)(2,1)} %stack.2), calls=%async_computation | async-start | bytes 16777216 | tf_op jit(solution)/shard_map/all_to_all | solution.py:29
  53.6 0.0 copy-done
  53.6 0.4 fusion
  54.0 0.0 copy-done.3
  54.0 0.0 copy-done.2
  54.0 725.9 %all-to-all-done = bf16[64,32,2048]{2,1,0:T(8,128)(2,1)} async-done(((bf16[64,32,2048]{2,1,0:T(8,128)(2,1)}), bf16[64,32,2048]{2,1,0:T(8,128)(2,1)}, u32[]{:S(2)}, u32[]{:S(2)}) %all-to-all-start) | async-done | bytes 8388640 | tf_op jit(solution)/shard_map/all_to_all | solution.py:29
  779.9 5.9 fusion.83
  785.8 6.5 copy.18
  792.4 2.6 fusion.20
  795.0 13.5 %collective-permute-start = (bf16[8,512]{1,0:T(8,128)(2,1)S(1)}, bf16[8,512]{1,0:T(8,128)(2,1)S(1)}, u32[]{:S(2)}, u32[]{:S(2)}) collective-permute-start(bf16[8,512]{1,0:T(8,128)(2,1)S(1)} %get-tuple-element.11), channel_id=1, source_target_pairs={{0,4},{4,8},{8,12},{12,16},{16,20},{20,24},{24,28},{28,32},{32,36}... | collective-permute-start | bytes 24584 | tf_op jit(solution)/shard_map/ppermute | solution.py:18
  808.5 3.2 collective-permute-start.1
  811.9 6.5 copy.22
  818.4 0.0 collective-permute-done
  818.4 0.0 collective-permute-done.1
  818.4 1.0 maximum_convert_fusion
  819.4 10.6 %convolution_convert_fusion.1 = bf16[384,2048]{1,0:T(8,128)(2,1)S(1)} fusion(bf16[2,512,2048]{2,1,0:T(8,128)(2,1)} %bitcast.95, bf16[2,1,512,512]{3,2,1,0:T(8,128)(2,1)} %param.9, f32[512]{0:T(512)S(1)} %bitcast.110, f32[400,1,512]{2,0,1:T(8,128)} %maximum_convert_fusion, f32[384]{0:T(512)S(1)} %subtract_convert_fusion, f32[]{:T(128)S(6)} %mul.373, ...), kind=kOutput, calls=%fused_computation.17 | convolution fusion | flops 1014497280 | bytes 16780864 | tf_op jit(solution)/shard_map/dot_general | solution.py:100
  830.0 0.8 broadcast_in_dim.4
  830.8 75.7 %all_to_all.15 = bf16[4,384,2048]{2,1,0:T(8,128)(2,1)S(1)} all-to-all(bf16[4,384,2048]{2,1,0:T(8,128)(2,1)S(1)} %broadcast_in_dim.4), channel_id=1, replica_groups=mesh['grp'=2,'sp'=64,'tp'=4] {'tp'}, dimensions={0} | all-to-all | bytes 12582912 | tf_op jit(solution)/shard_map/all_to_all | solution.py:43
  906.5 1.3 convert_reduce_fusion.1
  907.8 0.0 copy-start.1
  907.8 0.5 fusion.4
  908.3 1.6 copy-done.1
  910.0 1.0 fusion.23
  911.0 2.0 collective-permute-start.2
  913.0 2.6 collective-permute-start.3
  915.6 0.0 collective-permute-done.2
  915.6 2.4 collective-permute-done.3
  918.0 1.0 maximum_convert_fusion.1
  919.0 10.7 %convolution_convert_fusion = bf16[384,2048]{1,0:T(8,128)(2,1)S(1)} fusion(bf16[2,512,2048]{2,1,0:T(8,128)(2,1)} %bitcast.96, bf16[2,1,512,512]{3,2,1,0:T(8,128)(2,1)} %param.9, f32[512]{0:T(512)S(1)} %bitcast.109, f32[400,1,512]{2,0,1:T(8,128)} %maximum_convert_fusion.1, f32[384]{0:T(512)S(1)} %subtract_convert_fusion, f32[]{:T(128)S(6)} %mul.373, ...), kind=kOutput, calls=%fused_computation.16 | convolution fusion | flops 1014497280 | bytes 16780864 | tf_op jit(solution)/shard_map/dot_general | solution.py:100
  929.6 0.8 broadcast_in_dim.5
  930.4 73.3 %all_to_all.16 = bf16[4,384,2048]{2,1,0:T(8,128)(2,1)S(1)} all-to-all(bf16[4,384,2048]{2,1,0:T(8,128)(2,1)S(1)} %broadcast_in_dim.5), channel_id=1, replica_groups=mesh['grp'=2,'sp'=64,'tp'=4] {'tp'}, dimensions={0} | all-to-all | bytes 12582912 | tf_op jit(solution)/shard_map/all_to_all | solution.py:43
  1003.7 1.3 convert_reduce_fusion
  1005.0 1.6 fusion.7
  (8 shorter events, 0.1 us)
Async XLA Ops:
  6.0 47.6 %copy-start = (bf16[384,2048]{1,0:T(8,128)(2,1)S(1)}, bf16[384,2048]{1,0:T(8,128)(2,1)}, u32[]{:S(2)}) copy-start(bf16[384,2048]{1,0:T(8,128)(2,1)} %param.6) | copy-start | bytes 4718596
  6.0 48.0 %copy-start.3 = (f32[2,512]{1,0:T(2,128)S(1)}, f32[2,512]{1,0:T(2,128)}, u32[]{:S(2)}) copy-start(f32[2,512]{1,0:T(2,128)} %param.10) | copy-start | bytes 12292
  6.0 48.0 %copy-start.2 = (f32[2,2048]{1,0:T(2,128)S(1)}, f32[2,2048]{1,0:T(2,128)}, u32[]{:S(2)}) copy-start(f32[2,2048]{1,0:T(2,128)} %param.7) | copy-start | bytes 49156
  6.0 773.9 %all-to-all-start = ((bf16[64,32,2048]{2,1,0:T(8,128)(2,1)}), bf16[64,32,2048]{2,1,0:T(8,128)(2,1)}, u32[]{:S(2)}, u32[]{:S(2)}) async-start(bf16[64,32,2048]{2,1,0:T(8,128)(2,1)} %stack.2), calls=%async_computation | async-start | bytes 16777216 | tf_op jit(solution)/shard_map/all_to_all | solution.py:29
  795.0 23.4 %collective-permute-start = (bf16[8,512]{1,0:T(8,128)(2,1)S(1)}, bf16[8,512]{1,0:T(8,128)(2,1)S(1)}, u32[]{:S(2)}, u32[]{:S(2)}) collective-permute-start(bf16[8,512]{1,0:T(8,128)(2,1)S(1)} %get-tuple-element.11), channel_id=1, source_target_pairs={{0,4},{4,8},{8,12},{12,16},{16,20},{20,24},{24,28},{28,32},{32,36}... | collective-permute-start | bytes 24584 | tf_op jit(solution)/shard_map/ppermute | solution.py:18
  808.5 9.9 collective-permute-start.1
  907.8 2.2 copy-start.1
  911.0 4.6 collective-permute-start.2
  913.0 5.0 collective-permute-start.3
